TPU v7x, 32 devices: a whole 2x2x4 slice. The times are simulated.
32 devices in a mesh: sp: 8 (over z, x), tp: 4 (over y, core).
Axes of the slice: x: 2, y: 2, z: 4, core: 2. Of those that a mesh axis runs over, the one named last changes fastest.
Arguments:
- queries: bfloat16 [8192, 1024], P('sp', 'tp'), may hold values from -6 to 6, as said below
- key_rows: bfloat16 [8192, 1024], P('sp', 'tp'), may hold values from -6 to 6, as said below
- value_rows: bfloat16 [8192, 1024], P('sp', 'tp'), may hold values from -6 to 6
- lambdas: float32 [8], P('tp'), may hold values from 0.3 to 0.8
- head_gain: float32 [128], replicated, may hold values from 0.1 to 1.9
- out_weight: bfloat16 [1024, 2048], replicated, may hold values from -0.1875 to 0.1875
- stream: bfloat16 [8192, 2048], P(('sp', 'tp')), may hold values from -6 to 6
- ffn_gain: float32 [2048], replicated, may hold values from 0.1 to 1.9
- routes: int32 [8192, 2], P(('sp', 'tp')), may hold values from 0 to 7, all different within a row; in each aligned block of 256 rows (0 to 255, 256 to 511, ...) at most 80 rows name the same one
- route_weight: float32 [8192, 2], P(('sp', 'tp')), may hold values from 0.1 to 1
- gate_weight: bfloat16 [8, 2048, 5120], P('sp', None, 'tp'), may hold values from -0.125 to 0.125
- up_weight: bfloat16 [8, 2048, 5120], P('sp', None, 'tp'), may hold values from -0.125 to 0.125
- down_weight: bfloat16 [8, 5120, 2048], P('sp', 'tp'), may hold values from -0.078125 to 0.078125
Outputs:
- layer_out: bfloat16 [8192, 2048], P(('sp', 'tp'))
Inputs may be any that keep to these rules, and one draw needn't show every extreme that they name: Custom draw; the queries of a position meet only keys of the same or earlier positions. `key_rows`: custom draw. `routes`: each row names 2 different experts. In the 256 rows of one device no expert is named by more than 80 rows, and every draw reaches 80 on some device.
All inputs are finite; a program needn't handle non-finite values.
Results may differ from a plain program's by a relative error of at most 0.01.
Values may be sent and summed in bfloat16 or wider, within the bound.
A program may use at most 128 MiB of HBM per device.

v0:
```python
import functools
import math

import jax
import jax.numpy as jnp
from jax import lax
from jax.experimental import pallas as pl
from jax.experimental.pallas import tpu as pltpu
from jax.sharding import PartitionSpec as P

DH = 64


def moe_kernel(
    n,
    lanes,
    slots,
    out_ref,
    gate_hbm,
    up_hbm,
    down_hbm,
    back_ref,
    gate,
    up,
    down,
    rows,
    act,
    part,
    from_core,
    chip_sum,
    from_y,
    final,
    weight_sem,
    local_sem,
    a_send,
    a_recv,
    y_send,
    y_recv,
    c_send,
    c_recv,
    p_send,
    p_recv,
    q_send,
    q_recv,
    r_send,
    r_recv,
):
    sp = lax.axis_index("sp")
    tp = lax.axis_index("tp")
    core = tp % 2
    ypos = tp // 2
    other = ypos * 2 + (1 - core)
    half = lanes * slots

    def y_up(j):
        return ((ypos + j) % lanes) * 2 + core

    def y_down(j):
        return ((ypos + lanes - j) % lanes) * 2 + core

    def block(k, lane, j):
        return rows.at[k, pl.ds((lane * lanes + j) * slots, slots)]

    def remote(src, dst, send, recv, where):
        return pltpu.make_async_remote_copy(
            src_ref=src,
            dst_ref=dst,
            send_sem=send,
            recv_sem=recv,
            device_id=where,
            device_id_type=pl.DeviceIdType.MESH,
        )

    def exchange(k):
        goal = (sp + k) % n
        return remote(out_ref.at[goal], block(k, 0, 0), a_send.at[k], a_recv.at[k], (goal, tp))

    def across(k, j):
        return remote(
            block(k, 0, 0), block(k, 0, j), y_send.at[k, j], y_recv.at[k, j], (sp, y_up(j))
        )

    def relay(k, j):
        return remote(
            block(k, 0, j), block(k, 1, j), c_send.at[k, j], c_recv.at[k, j], (sp, other)
        )

    def core_part(k):
        return remote(
            part.at[k % 2, pl.ds(half, half)], from_core.at[k], p_send.at[k], p_recv.at[k], (sp, other)
        )

    def y_part(k, j):
        return remote(
            chip_sum.at[k, pl.ds(j * slots, slots)],
            from_y.at[k, pl.ds((j - 1) * slots, slots)],
            q_send.at[k, j],
            q_recv.at[k, j],
            (sp, y_down(j)),
        )

    def give_back(k):
        goal = (sp + n - k) % n
        return remote(final.at[k], back_ref.at[sp], r_send.at[k], r_recv.at[k], (goal, tp))

    weights = [
        pltpu.make_async_copy(a, b, weight_sem.at[i])
        for i, (a, b) in enumerate(((gate_hbm, gate), (up_hbm, up), (down_hbm, down)))
    ]
    for copy in weights:
        copy.start()
    own = pltpu.make_async_copy(out_ref.at[sp], block(0, 0, 0), local_sem.at[0])
    own.start()

    barrier = pltpu.get_barrier_semaphore()
    for k in range(1, n):
        pl.semaphore_signal(
            barrier, inc=1, device_id=((sp + k) % n, tp), device_id_type=pl.DeviceIdType.MESH
        )
    for k in range(1, 2 * lanes):
        pl.semaphore_signal(
            barrier,
            inc=1,
            device_id=(sp, (tp + k) % (2 * lanes)),
            device_id_type=pl.DeviceIdType.MESH,
        )
    pl.semaphore_wait(barrier, n + 2 * lanes - 2)

    @pl.loop(1, n)
    def _(k):
        exchange(k).start()

    def forward(k):
        for j in range(1, lanes):
            across(k, j).start()
        relay(k, 0).start()

    own.wait()
    forward(0)

    tile = math.gcd(gate.shape[1], 256)
    wide = math.gcd(down.shape[1], 256)

    @pl.loop(0, n + 3)
    def _(i):
        @pl.when(i < n - 1)
        def _():
            exchange(i + 1).wait_recv()
            forward(i + 1)

        @pl.when(i < n)
        def _():
            for j in range(1, lanes):
                across(i, j).wait_recv()
                relay(i, j).start()

        @pl.when((i >= 1) & (i < n + 1))
        def _():
            k = i - 1

            @pl.when(k == 0)
            def _():
                for copy in weights:
                    copy.wait()

            for j in range(lanes):
                relay(k, j).wait_recv()

            @pl.when(k >= 2)
            def _():
                core_part(k - 2).wait_send()

            @pl.loop(0, gate.shape[1] // tile)
            def _(f):
                cols = pl.ds(pl.multiple_of(f * tile, tile), tile)
                x = rows[k]
                g = jnp.dot(x, gate[:, cols], preferred_element_type=jnp.float32)
                u = jnp.dot(x, up[:, cols], preferred_element_type=jnp.float32)
                act[:, cols] = (g / (1.0 + jnp.exp(-g)) * u).astype(jnp.bfloat16)

            @pl.loop(0, down.shape[1] // wide)
            def _(d):
                cols = pl.ds(pl.multiple_of(d * wide, wide), wide)
                part[k % 2, :, cols] = jnp.dot(
                    act[...], down[:, cols], preferred_element_type=jnp.float32
                ).astype(jnp.bfloat16)

            core_part(k).start()

        @pl.when((i >= 2) & (i < n + 2))
        def _():
            k = i - 2
            core_part(k).wait_recv()

            @pl.loop(0, half // 16)
            def _(r):
                at = pl.ds(pl.multiple_of(r * 16, 16), 16)
                total = part[k % 2, at].astype(jnp.float32) + from_core[k, at].astype(jnp.float32)
                chip_sum[k, at] = total.astype(jnp.bfloat16)

            for j in range(1, lanes):
                y_part(k, j).start()

        @pl.when(i >= 3)
        def _():
            k = i - 3
            for j in range(1, lanes):
                y_part(k, j).wait_recv()

            @pl.loop(0, slots // 16)
            def _(r):
                at = pl.ds(pl.multiple_of(r * 16, 16), 16)
                total = chip_sum[k, at].astype(jnp.float32)
                for j in range(1, lanes):
                    here = pl.ds(pl.multiple_of((j - 1) * slots + r * 16, 16), 16)
                    total = total + from_y[k, here].astype(jnp.float32)
                final[k, at] = total.astype(jnp.bfloat16)

            @pl.when(k > 0)
            def _():
                give_back(k).start()

            @pl.when(k == 0)
            def _():
                pltpu.make_async_copy(final.at[0], back_ref.at[sp], local_sem.at[1]).start()

    pltpu.make_async_copy(final.at[0], back_ref.at[sp], local_sem.at[1]).wait()
    for k in (n - 2, n - 1):
        core_part(k).wait_send()

    @pl.loop(0, n)
    def _(k):
        @pl.when(k > 0)
        def _():
            exchange(k).wait_send()
            give_back(k).wait_send()
            give_back(k).wait_recv()

        for j in range(1, lanes):
            across(k, j).wait_send()
            y_part(k, j).wait_send()
        for j in range(lanes):
            relay(k, j).wait_send()


def exchange_and_apply(outgoing, gate_local, up_local, down_local):
    n, slots, width = outgoing.shape
    lanes = lax.axis_size("tp") // 2
    hidden = gate_local.shape[1]
    kind = jnp.bfloat16
    dma = pltpu.SemaphoreType.DMA
    flops = 6 * n * lanes * 2 * slots * width * hidden
    return pl.pallas_call(
        functools.partial(moe_kernel, n, lanes, slots),
        out_shape=jax.ShapeDtypeStruct((n, slots, width), kind),
        in_specs=[pl.BlockSpec(memory_space=pltpu.VMEM)]
        + [pl.BlockSpec(memory_space=pl.ANY)] * 3,
        out_specs=pl.BlockSpec(memory_space=pltpu.VMEM),
        scratch_shapes=[
            pltpu.VMEM((width, hidden), kind),
            pltpu.VMEM((width, hidden), kind),
            pltpu.VMEM((hidden, width), kind),
            pltpu.VMEM((n, 2 * lanes * slots, width), kind),
            pltpu.VMEM((2 * lanes * slots, hidden), kind),
            pltpu.VMEM((2, 2 * lanes * slots, width), kind),
            pltpu.VMEM((n, lanes * slots, width), kind),
            pltpu.VMEM((n, lanes * slots, width), kind),
            pltpu.VMEM((n, max(1, lanes - 1) * slots, width), kind),
            pltpu.VMEM((n, slots, width), kind),
            dma((3,)),
            dma((2,)),
            dma((n,)),
            dma((n,)),
            dma((n, lanes)),
            dma((n, lanes)),
            dma((n, lanes)),
            dma((n, lanes)),
            dma((n,)),
            dma((n,)),
            dma((n, lanes)),
            dma((n, lanes)),
            dma((n,)),
            dma((n,)),
        ],
        compiler_params=pltpu.CompilerParams(
            collective_id=0, has_side_effects=True, vmem_limit_bytes=67000000
        ),
        cost_estimate=pl.CostEstimate(
            flops=flops, bytes_accessed=6 * width * hidden, transcendentals=0
        ),
    )(outgoing, gate_local, up_local, down_local)


def attention_kernel(
    n,
    across_x,
    heads,
    tall,
    q_ref,
    kv_hbm,
    lam_ref,
    gain_ref,
    o_ref,
    kv,
    masked_q,
    maxima,
    accum,
    own_sem,
    z_send,
    z_recv,
    x_send,
    x_recv,
):
    sp = lax.axis_index("sp")
    tp = lax.axis_index("tp")
    z = sp // across_x
    x = sp % across_x
    deep = n // across_x
    length = q_ref.shape[0]
    wide = 2 * DH
    own = pltpu.make_async_copy(kv_hbm, kv.at[0], own_sem.at[0])
    own.start()

    def signal(where):
        pl.semaphore_signal(
            pltpu.get_barrier_semaphore(),
            inc=1,
            device_id=(where, tp),
            device_id_type=pl.DeviceIdType.MESH,
        )

    signal(((z + 1) % deep) * across_x + x)
    signal(((z + deep - 1) % deep) * across_x + x)
    for r in range(1, across_x):
        signal(z * across_x + (x + r) % across_x)
    pl.semaphore_wait(pltpu.get_barrier_semaphore(), across_x + 1)

    def upward(d):
        return pltpu.make_async_remote_copy(
            src_ref=kv.at[d * across_x],
            dst_ref=kv.at[(d + 1) * across_x],
            send_sem=z_send.at[d],
            recv_sem=z_recv.at[d + 1],
            device_id=(((z + 1) % deep) * across_x + x, tp),
            device_id_type=pl.DeviceIdType.MESH,
        )

    def arrived_z(d):
        return pltpu.make_async_remote_copy(
            src_ref=kv.at[(d - 1) * across_x],
            dst_ref=kv.at[d * across_x],
            send_sem=z_send.at[d - 1],
            recv_sem=z_recv.at[d],
            device_id=(((z + 1) % deep) * across_x + x, tp),
            device_id_type=pl.DeviceIdType.MESH,
        )

    def sideways(d, r):
        return pltpu.make_async_remote_copy(
            src_ref=kv.at[d * across_x],
            dst_ref=kv.at[d * across_x + r],
            send_sem=x_send.at[d * across_x + r],
            recv_sem=x_recv.at[d * across_x + r],
            device_id=(z * across_x + (x + r) % across_x, tp),
            device_id_type=pl.DeviceIdType.MESH,
        )

    own.wait()

    @pl.when(z + 1 < deep)
    def _():
        upward(0).start()

    for r in range(1, across_x):
        @pl.when(x + r < across_x)
        def _(r=r):
            sideways(0, r).start()

    lane = lax.broadcasted_iota(jnp.int32, (length, wide), 1)
    for h in range(heads):
        scaled = q_ref[:, h * wide : (h + 1) * wide].astype(jnp.float32) * DH ** (-0.5)
        for m in range(2):
            keep = (lane >= m * DH) & (lane < (m + 1) * DH)
            masked_q[2 * h + m] = jnp.where(keep, scaled, 0.0).astype(jnp.bfloat16)

    def attend(slot, first):
        @pl.loop(0, length // tall)
        def _(i):
            at = pl.ds(pl.multiple_of(i * tall, tall), tall)
            for h in range(heads):
                keys = kv[slot, :, h * wide : (h + 1) * wide]
                values = kv[slot, :, (heads + h) * wide : (heads + h + 1) * wide]
                values = jnp.concatenate([values, jnp.ones_like(values)], axis=1)
                for m in range(2):
                    row = 2 * h + m
                    scores = lax.dot_general(
                        masked_q[row, at],
                        keys,
                        (((1,), (1,)), ((), ())),
                        preferred_element_type=jnp.float32,
                    )
                    if first:
                        q_pos = i * tall + lax.broadcasted_iota(jnp.int32, scores.shape, 0)
                        k_pos = lax.broadcasted_iota(jnp.int32, scores.shape, 1)
                        scores = jnp.where(k_pos <= q_pos, scores, -1e30)
                    top = jnp.max(scores, axis=1, keepdims=True)
                    if not first:
                        old = maxima[row, at, 0:1]
                        top = jnp.maximum(old, top)
                    weights = jnp.exp(scores - top).astype(jnp.bfloat16)
                    mixed = jnp.dot(weights, values, preferred_element_type=jnp.float32)
                    if not first:
                        mixed = accum[row, at] * jnp.exp(old - top) + mixed
                    accum[row, at] = mixed
                    maxima[row, at] = jnp.broadcast_to(top, (tall, wide))

    attend(0, True)

    @pl.loop(1, n)
    def _(t):
        d = t // across_x
        r = t % across_x

        @pl.when((r == 1) & (d + 1 < deep) & (z >= d + 1))
        def _():
            arrived_z(d + 1).wait_recv()

            @pl.when(z + 1 < deep)
            def _():
                upward(d + 1).start()

            for k in range(1, across_x):
                sideways(d + 1, k).start()

        valid = (z >= d) & ((d > 0) | (x >= r))

        @pl.when(valid & (r > 0))
        def _():
            sideways(d, r).wait_recv()

        @pl.when(valid)
        def _():
            attend(t, False)

    @pl.loop(0, length // tall)
    def _(i):
        at = pl.ds(pl.multiple_of(i * tall, tall), tall)
        for h in range(heads):
            one = accum[2 * h, at, 0:wide] / accum[2 * h, at, wide : 2 * wide]
            two = accum[2 * h + 1, at, 0:wide] / accum[2 * h + 1, at, wide : 2 * wide]
            contrast = one - lam_ref[h : h + 1, :] * two
            square = jnp.mean(contrast * contrast, axis=1, keepdims=True)
            contrast = contrast * lax.rsqrt(square + 1e-05) * gain_ref[...]
            o_ref[at, h * wide : (h + 1) * wide] = contrast.astype(jnp.bfloat16)

    for d in range(deep):
        @pl.when((z >= d) & (z + 1 < deep))
        def _(d=d):
            upward(d).wait_send()

        for r in range(1, across_x):
            @pl.when((z >= d) & ((d > 0) | (x + r < across_x)))
            def _(d=d, r=r):
                sideways(d, r).wait_send()


def attention(queries, key_rows, value_rows, lambdas, head_gain):
    n = lax.axis_size("sp")
    across_x = 2 ** (int(math.log2(n)) // 2)
    length, columns = queries.shape
    wide = 2 * DH
    heads = columns // wide
    kind = jnp.bfloat16
    dma = pltpu.SemaphoreType.DMA
    deep = n // across_x
    vmem = pl.BlockSpec(memory_space=pltpu.VMEM)
    return pl.pallas_call(
        functools.partial(attention_kernel, n, across_x, heads, math.gcd(length, 256)),
        out_shape=jax.ShapeDtypeStruct((length, columns), kind),
        in_specs=[vmem, pl.BlockSpec(memory_space=pl.ANY), vmem, vmem],
        out_specs=vmem,
        scratch_shapes=[
            pltpu.VMEM((n, length, 2 * columns), kind),
            pltpu.VMEM((2 * heads, length, wide), kind),
            pltpu.VMEM((2 * heads, length, wide), jnp.float32),
            pltpu.VMEM((2 * heads, length, 2 * wide), jnp.float32),
            dma((1,)),
            dma((deep + 1,)),
            dma((deep + 1,)),
            dma((n,)),
            dma((n,)),
        ],
        compiler_params=pltpu.CompilerParams(
            collective_id=1, has_side_effects=True, vmem_limit_bytes=60000000
        ),
    )(
        queries,
        jnp.concatenate([key_rows, value_rows], axis=1),
        jnp.broadcast_to(lambdas[:, None], (heads, wide)),
        head_gain[None, :],
    )


def local(
    queries,
    key_rows,
    value_rows,
    lambdas,
    head_gain,
    out_weight,
    stream,
    ffn_gain,
    routes,
    route_weight,
    gate_weight,
    up_weight,
    down_weight,
):
    heads_out = attention(queries, key_rows, value_rows, lambdas, head_gain)
    heads_local = lax.all_to_all(heads_out, "tp", split_axis=0, concat_axis=1, tiled=True)
    attended = stream.astype(jnp.float32) + jnp.dot(
        heads_local, out_weight, preferred_element_type=jnp.float32
    )
    normed = (
        attended
        * lax.rsqrt(jnp.mean(attended * attended, axis=-1, keepdims=True) + 1e-06)
        * ffn_gain
    ).astype(jnp.bfloat16)
    rows_local = normed.shape[0]
    width = normed.shape[1]
    top_count = routes.shape[1]
    sp_size = lax.axis_size("sp")
    experts = sp_size * gate_weight.shape[0]
    slots = max(2, (rows_local * top_count * 5 + 4 * experts - 1) // (4 * experts))
    slots = -(-slots // 16) * 16
    flat_routes = routes.reshape(-1)
    onehot = (flat_routes[:, None] == jnp.arange(experts, dtype=jnp.int32)[None, :]).astype(
        jnp.int32
    )
    before = jnp.cumsum(onehot, axis=0) - onehot
    slot = jnp.sum(before * onehot, axis=1)
    target = flat_routes * slots + slot
    placed = (target[:, None] == jnp.arange(experts * slots, dtype=jnp.int32)[None, :]).astype(
        jnp.float32
    )
    placed = placed.reshape(rows_local, top_count, experts * slots)
    dispatch = jnp.transpose(jnp.sum(placed, axis=1)).astype(jnp.bfloat16)
    combine = jnp.einsum("tk,tks->ts", route_weight, placed, precision=lax.Precision.HIGHEST)
    outgoing = (
        jnp.dot(dispatch, normed, preferred_element_type=jnp.float32)
        .astype(jnp.bfloat16)
        .reshape(experts, slots, width)
    )
    gate_local = gate_weight[0]
    up_local = up_weight[0]
    down_local = down_weight[0]
    returned = exchange_and_apply(outgoing, gate_local, up_local, down_local).reshape(
        experts * slots, width
    )
    routed = jnp.dot(combine, returned.astype(jnp.float32), precision=lax.Precision.HIGHEST)
    return (attended + routed).astype(jnp.bfloat16)


def solution(mesh):
    placed = (
        P("sp", "tp"),
        P("sp", "tp"),
        P("sp", "tp"),
        P("tp"),
        P(),
        P(),
        P(("sp", "tp"), None),
        P(),
        P(("sp", "tp"), None),
        P(("sp", "tp"), None),
        P("sp", None, "tp"),
        P("sp", None, "tp"),
        P("sp", "tp", None),
    )
    return jax.shard_map(
        local, mesh=mesh, in_specs=placed, out_specs=P(("sp", "tp"), None), check_vma=False
    )
```

profile of v0, /device:TPU:0, one launch (start us, length us, event | category | flops | bytes accessed | tf_op | source)
XLA Modules:
  0.0 306.7 jit_solution(7584911827541581031)
XLA Ops:
  0.0 2.3 pad_maximum_fusion.kv_hbm
  2.3 0.7 broadcast_in_dim.4.lam_ref
  2.9 29.6 %shard_map.127 = bf16[1024,256]{1,0:T(8,128)(2,1)} custom-call(bf16[1024,256]{1,0:T(8,128)(2,1)} %q_ref.1, bf16[1024,512]{1,0:T(8,128)(2,1)} %pad_maximum_fusion.kv_hbm, f32[2,128]{1,0:T(2,128)} %broadcast_in_dim.4.lam_ref, f32[1,128]{1,0:T(1,128)} %bitcast.32), custom_call_target="tpu_custom_call" | custom-call | tf_op jit(solution)/shard_map/pallas_call | solution.py:477
  32.5 0.0 copy-start.4
  32.5 2.0 copy.26
  34.6 3.7 %all-to-all-start = ((bf16[4,256,256]{1,2,0:T(8,128)(2,1)}), bf16[4,256,256]{1,2,0:T(8,128)(2,1)S(1)}, u32[]{:S(2)}, u32[]{:S(2)}) async-start(bf16[4,256,256]{1,2,0:T(8,128)(2,1)} %copy.26), calls=%async_computation | async-start | bytes 1048576 | tf_op jit(solution)/shard_map/all_to_all | solution.py:520
  38.2 0.1 copy.27
  38.4 0.1 eq.44
  38.5 0.1 eq.40
  38.7 1.1 reduce-window.6
  39.8 0.2 slice_reduce_fusion
  40.1 0.1 fusion.9
  40.2 0.1 reduce_sum.30
  40.3 0.1 copy.29
  40.4 0.3 iota_compare_fusion
  40.7 0.1 copy.31
  40.8 0.2 convert_reduce_fusion
  41.0 0.0 copy-start.1
  41.1 3.9 %fusion = f32[256,1,640]{2,1,0:T(1,128)} fusion(f32[256,2,1]{1,2,0:T(1,128)S(1)} %copy.31, pred[256,2,640]{2,0,1:T(32,128)(4,1)S(1)} %iota_compare_fusion), kind=kOutput, calls=%fused_computation.2 | convolution fusion | flops 3932160 | bytes 985088 | tf_op jit(solution)/shard_map/tk,tks->ts/dot_general | solution.py:548
  45.0 1.8 all-to-all-done
  46.8 3.6 %multiply_reduce_fusion = (f32[256]{0:T(256)S(1)}, f32[256,2048]{1,0:T(8,128)S(1)}) fusion(bf16[256,1024]{0,1:T(8,128)(2,1)S(1)} %bitcast.27, bf16[1024,2048]{1,0:T(8,128)(2,1)} %param.18, bf16[256,2048]{1,0:T(8,128)(2,1)S(1)} %copy-done.1), kind=kOutput, calls=%fused_computation.7 | convolution fusion | flops 1075838720 | bytes 7865344 | tf_op jit(solution)/shard_map/dot_general | solution.py:521
  50.4 2.5 convolution_convert_fusion
  53.0 247.6 %shard_map.128 = bf16[8,80,2048]{2,1,0:T(8,128)(2,1)} custom-call(bf16[8,80,2048]{2,1,0:T(8,128)(2,1)} %bitcast.29, bf16[2048,1280]{1,0:T(8,128)(2,1)} %bitcast.33, bf16[2048,1280]{1,0:T(8,128)(2,1)} %bitcast.34, bf16[1280,2048]{1,0:T(8,128)(2,1)} %bitcast.35), custom_call_target="tpu_custom_call" | custom-call | flops 40265318400 | bytes 15728640 | tf_op jit(solution)/shard_map/pallas_call | solution.py:253
  300.6 6.2 %fusion.2 = bf16[256,2048]{1,0:T(8,128)(2,1)} fusion(f32[256,2048]{1,0:T(8,128)} %copy-done, bf16[640,2048]{1,0:T(8,128)(2,1)} %bitcast.28, f32[256,1,640]{2,1,0:T(1,128)} %fusion), kind=kOutput, calls=%fused_computation.5 | convolution fusion | flops 4027580416 | bytes 6422528 | tf_op jit(solution)/shard_map/dot_general | solution.py:560
  (15 shorter events, 0.1 us)
Async XLA Ops:
  0.0 2.3 copy-start.5
  2.9 35.3 %copy-start.3 = (s32[256,2]{0,1:T(2,128)S(1)}, s32[256,2]{0,1:T(2,128)}, u32[]{:S(2)}) copy-start(s32[256,2]{0,1:T(2,128)} %param.21) | copy-start | bytes 6148
  32.5 8.2 %copy-start.4 = (f32[256,2]{0,1:T(2,128)S(1)}, f32[256,2]{0,1:T(2,128)}, u32[]{:S(2)}) copy-start(f32[256,2]{0,1:T(2,128)} %param.22) | copy-start | bytes 6148
  34.6 12.3 %all-to-all-start = ((bf16[4,256,256]{1,2,0:T(8,128)(2,1)}), bf16[4,256,256]{1,2,0:T(8,128)(2,1)S(1)}, u32[]{:S(2)}, u32[]{:S(2)}) async-start(bf16[4,256,256]{1,2,0:T(8,128)(2,1)} %copy.26), calls=%async_computation | async-start | bytes 1048576 | tf_op jit(solution)/shard_map/all_to_all | solution.py:520
  41.0 5.8 %copy-start.1 = (bf16[256,2048]{1,0:T(8,128)(2,1)S(1)}, bf16[256,2048]{1,0:T(8,128)(2,1)}, u32[]{:S(2)}) copy-start(bf16[256,2048]{1,0:T(8,128)(2,1)} %param.19) | copy-start | bytes 3145732
  46.8 3.6 %copy-start.2 = (f32[2048]{0:T(1024)S(1)}, f32[2048]{0:T(1024)}, u32[]{:S(2)}) copy-start(f32[2048]{0:T(1024)} %param.20) | copy-start | bytes 24580
  50.4 2.5 copy-start
where the time goes:
time: 307 us
  Pallas kernels  277 us (90%)
  matrix products  16.2 us (5%)
  other arithmetic  4 us (1%)
  local copies, waits for them, and re-layouts  3.72 us (1%)
  starting transfers between devices  3.65 us (1%)
    pallas_call x1, Pallas kernels, exchange_and_apply(): pl.pallas_call(functools.partial(moe_kernel, n, lanes, slots), out_shape=...  248 us
    pallas_call x1, Pallas kernels, attention(): pl.pallas_call(functools.partial(attention_kernel, n, across_x, heads, ma...  29.6 us
    dot_general x1, matrix products, local(): jnp.dot(combine, returned.astype(jnp.float32), precision=lax.Precision.HI...  6.17 us
  transfers between devices with their start and end apart: 1, of which 1 were waited for; matrix products, arithmetic and copies ran while one was open for 2% of the time, Pallas kernels for 0%

commit v1 on v0

--- a/solution.py
+++ b/solution.py
@@ -293,210 +293,356 @@
 
 def attention_kernel(
     n,
-    across_x,
+    group,
     heads,
-    tall,
+    post,
     q_ref,
-    kv_hbm,
+    k_ref,
+    v_ref,
     lam_ref,
     gain_ref,
     o_ref,
-    kv,
+    keys,
+    values,
+    turned,
+    asked,
     masked_q,
     maxima,
     accum,
-    own_sem,
-    z_send,
-    z_recv,
-    x_send,
-    x_recv,
+    done,
+    lam,
+    kv_send,
+    k_recv,
+    v_recv,
+    side_send,
+    core_send,
+    q_send,
+    q_recv,
+    lam_send,
+    lam_recv,
+    o_send,
+    o_recv,
 ):
     sp = lax.axis_index("sp")
     tp = lax.axis_index("tp")
-    z = sp // across_x
-    x = sp % across_x
-    deep = n // across_x
+    tp_size = lax.axis_size("tp")
+    core = tp % 2
+    plane = tp // 2
+    other = plane * 2 + (1 - core)
+    in_plane = 2 * heads
+    head = sp // group
+    seat = sp % group
+    source_core = head // heads
+    is_source = core == source_core
     length = q_ref.shape[0]
     wide = 2 * DH
-    own = pltpu.make_async_copy(kv_hbm, kv.at[0], own_sem.at[0])
-    own.start()
-
-    def signal(where):
+    chunks = 4 * group
+    per_block = chunks // n
+    size = length // per_block
+    place = seat * 2 + core
+    chunk_of = (place, chunks - 1 - place)
+    parts = size // post
+
+    def remote(src, dst, send, recv, where):
+        return pltpu.make_async_remote_copy(
+            src_ref=src,
+            dst_ref=dst,
+            send_sem=send,
+            recv_sem=recv,
+            device_id=where,
+            device_id_type=pl.DeviceIdType.MESH,
+        )
+
+    barrier = pltpu.get_barrier_semaphore()
+    everyone = n * tp_size
+    me = sp * tp_size + tp
+
+    @pl.loop(1, everyone)
+    def _(k):
+        to = (me + k) % everyone
         pl.semaphore_signal(
-            pltpu.get_barrier_semaphore(),
+            barrier,
             inc=1,
-            device_id=(where, tp),
+            device_id=(to // tp_size, to % tp_size),
             device_id_type=pl.DeviceIdType.MESH,
         )
 
-    signal(((z + 1) % deep) * across_x + x)
-    signal(((z + deep - 1) % deep) * across_x + x)
-    for r in range(1, across_x):
-        signal(z * across_x + (x + r) % across_x)
-    pl.semaphore_wait(pltpu.get_barrier_semaphore(), across_x + 1)
-
-    def upward(d):
-        return pltpu.make_async_remote_copy(
-            src_ref=kv.at[d * across_x],
-            dst_ref=kv.at[(d + 1) * across_x],
-            send_sem=z_send.at[d],
-            recv_sem=z_recv.at[d + 1],
-            device_id=(((z + 1) % deep) * across_x + x, tp),
-            device_id_type=pl.DeviceIdType.MESH,
-        )
-
-    def arrived_z(d):
-        return pltpu.make_async_remote_copy(
-            src_ref=kv.at[(d - 1) * across_x],
-            dst_ref=kv.at[d * across_x],
-            send_sem=z_send.at[d - 1],
-            recv_sem=z_recv.at[d],
-            device_id=(((z + 1) % deep) * across_x + x, tp),
-            device_id_type=pl.DeviceIdType.MESH,
-        )
-
-    def sideways(d, r):
-        return pltpu.make_async_remote_copy(
-            src_ref=kv.at[d * across_x],
-            dst_ref=kv.at[d * across_x + r],
-            send_sem=x_send.at[d * across_x + r],
-            recv_sem=x_recv.at[d * across_x + r],
-            device_id=(z * across_x + (x + r) % across_x, tp),
-            device_id_type=pl.DeviceIdType.MESH,
-        )
-
-    own.wait()
-
-    @pl.when(z + 1 < deep)
+    pl.semaphore_wait(barrier, everyone - 1)
+
+    def columns(h):
+        return pl.ds(pl.multiple_of(h * wide, wide), wide)
+
+    def turn_of(k):
+        return jnp.where(head % 2 == 1, heads - 1 - k, k)
+
+    def q_piece(k, i):
+        h = turn_of(k)
+        chunk = sp * per_block + i
+        late = chunk >= 2 * group
+        spot = jnp.where(late, chunks - 1 - chunk, chunk)
+        slot = jnp.where(late, 1, 0)
+        goal = (core * heads + h) * group + spot // 2
+        goal_core = spot % 2
+        src = q_ref.at[pl.ds(i * size, size), columns(h)]
+        here = (goal == sp) & (goal_core == core)
+        sem = q_send.at[k * per_block + i]
+        far = remote(
+            src, asked.at[slot], sem, q_recv.at[slot], (goal, plane * 2 + goal_core)
+        )
+        near = pltpu.make_async_copy(src, asked.at[slot], q_recv.at[slot])
+        return here, far, near
+
+    def kv_piece(k, which):
+        h = turn_of(k)
+        goal_head = core * heads + h
+        here = goal_head == head
+        src = k_ref.at[:, columns(h)] if which == 0 else turned.at[h]
+        dst = (keys if which == 0 else values).at[sp]
+        recv = (k_recv if which == 0 else v_recv).at[sp]
+        far = remote(
+            src, dst, kv_send.at[k * 2 + which], recv, (goal_head * group + seat, tp)
+        )
+        near = pltpu.make_async_copy(src, dst, recv)
+        return here, far, near
+
+    def launch(here, far, near):
+        @pl.when(here)
+        def _():
+            near.start()
+
+        @pl.when(jnp.logical_not(here))
+        def _():
+            far.start()
+
+    pieces = [q_piece(k, i) for k in range(heads) for i in range(per_block)]
+    pieces.append(kv_piece(0, 0))
+    for piece in pieces:
+        launch(*piece)
+    for h in range(heads):
+        block = v_ref[:, h * wide : (h + 1) * wide].astype(jnp.float32)
+        turned[h] = jnp.transpose(block).astype(jnp.bfloat16)
+    later = [kv_piece(0, 1)] + [kv_piece(k, which) for k in range(1, heads) for which in range(2)]
+    for piece in later:
+        launch(*piece)
+    pieces += later
+    for row in range(4):
+        accum[row] = jnp.zeros(accum.shape[1:], jnp.float32)
+        maxima[row] = jnp.full(maxima.shape[1:], -1e30, jnp.float32)
+
+    def lam_copy():
+        return remote(
+            lam_ref.at[head % heads], lam, lam_send.at[0], lam_recv.at[0], (sp, other)
+        )
+
+    @pl.when(is_source)
     def _():
-        upward(0).start()
-
-    for r in range(1, across_x):
-        @pl.when(x + r < across_x)
-        def _(r=r):
-            sideways(0, r).start()
-
-    lane = lax.broadcasted_iota(jnp.int32, (length, wide), 1)
-    for h in range(heads):
-        scaled = q_ref[:, h * wide : (h + 1) * wide].astype(jnp.float32) * DH ** (-0.5)
+        lam_copy().start()
+
+    lane = lax.broadcasted_iota(jnp.int32, (wide, size), 0)
+    for slot in range(2):
+        pltpu.make_async_copy(asked.at[slot], asked.at[slot], q_recv.at[slot]).wait()
+        turn = jnp.transpose(asked[slot].astype(jnp.float32)) * (DH ** (-0.5) * math.log2(math.e))
+        high = turn.astype(jnp.bfloat16)
+        low = (turn - high.astype(jnp.float32)).astype(jnp.bfloat16)
         for m in range(2):
             keep = (lane >= m * DH) & (lane < (m + 1) * DH)
-            masked_q[2 * h + m] = jnp.where(keep, scaled, 0.0).astype(jnp.bfloat16)
-
-    def attend(slot, first):
-        @pl.loop(0, length // tall)
-        def _(i):
-            at = pl.ds(pl.multiple_of(i * tall, tall), tall)
-            for h in range(heads):
-                keys = kv[slot, :, h * wide : (h + 1) * wide]
-                values = kv[slot, :, (heads + h) * wide : (heads + h + 1) * wide]
-                values = jnp.concatenate([values, jnp.ones_like(values)], axis=1)
-                for m in range(2):
-                    row = 2 * h + m
-                    scores = lax.dot_general(
-                        masked_q[row, at],
-                        keys,
-                        (((1,), (1,)), ((), ())),
-                        preferred_element_type=jnp.float32,
-                    )
-                    if first:
-                        q_pos = i * tall + lax.broadcasted_iota(jnp.int32, scores.shape, 0)
-                        k_pos = lax.broadcasted_iota(jnp.int32, scores.shape, 1)
-                        scores = jnp.where(k_pos <= q_pos, scores, -1e30)
-                    top = jnp.max(scores, axis=1, keepdims=True)
-                    if not first:
-                        old = maxima[row, at, 0:1]
-                        top = jnp.maximum(old, top)
-                    weights = jnp.exp(scores - top).astype(jnp.bfloat16)
-                    mixed = jnp.dot(weights, values, preferred_element_type=jnp.float32)
-                    if not first:
-                        mixed = accum[row, at] * jnp.exp(old - top) + mixed
-                    accum[row, at] = mixed
-                    maxima[row, at] = jnp.broadcast_to(top, (tall, wide))
-
-    attend(0, True)
-
-    @pl.loop(1, n)
-    def _(t):
-        d = t // across_x
-        r = t % across_x
-
-        @pl.when((r == 1) & (d + 1 < deep) & (z >= d + 1))
-        def _():
-            arrived_z(d + 1).wait_recv()
-
-            @pl.when(z + 1 < deep)
-            def _():
-                upward(d + 1).start()
-
-            for k in range(1, across_x):
-                sideways(d + 1, k).start()
-
-        valid = (z >= d) & ((d > 0) | (x >= r))
-
-        @pl.when(valid & (r > 0))
-        def _():
-            sideways(d, r).wait_recv()
-
-        @pl.when(valid)
-        def _():
-            attend(t, False)
-
-    @pl.loop(0, length // tall)
-    def _(i):
-        at = pl.ds(pl.multiple_of(i * tall, tall), tall)
-        for h in range(heads):
-            one = accum[2 * h, at, 0:wide] / accum[2 * h, at, wide : 2 * wide]
-            two = accum[2 * h + 1, at, 0:wide] / accum[2 * h + 1, at, wide : 2 * wide]
-            contrast = one - lam_ref[h : h + 1, :] * two
-            square = jnp.mean(contrast * contrast, axis=1, keepdims=True)
-            contrast = contrast * lax.rsqrt(square + 1e-05) * gain_ref[...]
-            o_ref[at, h * wide : (h + 1) * wide] = contrast.astype(jnp.bfloat16)
-
-    for d in range(deep):
-        @pl.when((z >= d) & (z + 1 < deep))
-        def _(d=d):
-            upward(d).wait_send()
-
-        for r in range(1, across_x):
-            @pl.when((z >= d) & ((d > 0) | (x + r < across_x)))
-            def _(d=d, r=r):
-                sideways(d, r).wait_send()
+            masked_q[slot * 2 + m, 0:wide] = jnp.where(keep, high, jnp.zeros_like(high))
+            masked_q[slot * 2 + m, wide : 2 * wide] = jnp.where(keep, low, jnp.zeros_like(low))
+
+    def source_of(w):
+        t = w // group
+        r = w % group
+        b = (head % 2 + t % 2) % 2 + 2 * ((head // 2 + t // 2) % 2)
+        return b * group + (seat + r) % group, r
+
+    def sideways(s, r, which):
+        buf = (keys if which == 0 else values).at[s]
+        recv = (k_recv if which == 0 else v_recv).at[s]
+        goal = head * group + (seat + r) % group
+        return remote(buf, buf, side_send.at[s, r, which], recv, (goal, tp))
+
+    def to_core(s, which):
+        buf = (keys if which == 0 else values).at[s]
+        recv = (k_recv if which == 0 else v_recv).at[s]
+        return remote(buf, buf, core_send.at[s, which], recv, (sp, other))
+
+    def receive(w):
+        s, r = source_of(w)
+        for which in range(2):
+            to_core(s, which).wait_recv()
+
+            @pl.when(is_source)
+            def _(which=which):
+                @pl.when(r == 0)
+                def _():
+                    for k in range(1, group):
+                        sideways(s, k, which).start()
+
+                to_core(s, which).start()
+
+    tall = math.gcd(length, 512)
+
+    def attend(slot, s, chunk, diagonal):
+        for first in range(0, length, tall):
+            k = keys[s, first : first + tall]
+            k = jnp.concatenate([k, k], axis=1)
+            v = values[s, :, first : first + tall]
+            v = jnp.concatenate([v, jnp.ones((16, tall), jnp.bfloat16)], axis=0)
+            for m in range(2):
+                row = slot * 2 + m
+                scores = jnp.dot(k, masked_q[row], preferred_element_type=jnp.float32)
+                if diagonal:
+                    k_pos = s * length + first + lax.broadcasted_iota(jnp.int32, scores.shape, 0)
+                    q_pos = chunk * size + lax.broadcasted_iota(jnp.int32, scores.shape, 1)
+                    scores = jnp.where(k_pos <= q_pos, scores, -1e30)
+                old = maxima[row, 0:1]
+                top = jnp.maximum(jnp.max(scores, axis=0, keepdims=True), old)
+                weights = jnp.exp2(scores - top).astype(jnp.bfloat16)
+                mixed = jnp.dot(v, weights, preferred_element_type=jnp.float32)
+                accum[row] = accum[row] * jnp.exp2(old - top) + mixed
+                maxima[row] = jnp.broadcast_to(top, maxima.shape[1:])
+
+    def step(slot, w):
+        s, _ = source_of(w)
+        chunk = jnp.where(slot == 0, chunk_of[0], chunk_of[1])
+        block = chunk // per_block
+
+        @pl.when(s == block)
+        def _():
+            attend(slot, s, chunk, True)
+
+        @pl.when(s < block)
+        def _():
+            attend(slot, s, chunk, False)
+
+    receive(0)
+
+    @pl.loop(0, n)
+    def _(w):
+        @pl.when(w + 1 < n)
+        def _():
+            receive(w + 1)
+
+        @pl.when(w < n - group)
+        def _():
+            @pl.loop(0, 2)
+            def _(slot):
+                step(slot, w)
+
+    @pl.when(is_source)
+    def _():
+        lam[...] = lam_ref[head % heads]
+
+    @pl.when(jnp.logical_not(is_source))
+    def _():
+        lam_copy().wait_recv()
+
+    full_head = plane * in_plane + head
+
+    def hand_over(slot, i):
+        chunk = chunk_of[slot]
+        goal = chunk // per_block
+        goal_tp = (chunk % per_block) * parts + i
+        here = (goal == sp) & (goal_tp == tp)
+        src = done.at[slot, pl.ds(i * post, post)]
+        dst = o_ref.at[:, pl.ds(pl.multiple_of(full_head * wide, wide), wide)]
+        far = remote(src, dst, o_send.at[slot * parts + i], o_recv.at[full_head], (goal, goal_tp))
+        near = pltpu.make_async_copy(src, dst, o_recv.at[full_head])
+        return here, far, near
+
+    handed = [[hand_over(slot, i) for i in range(parts)] for slot in range(2)]
+
+    @pl.loop(0, 2)
+    def _(slot):
+        @pl.loop(n - group, n)
+        def _(w):
+            step(slot, w)
+
+        one = accum[slot * 2, 0:wide] * (1.0 / accum[slot * 2, wide : wide + 1])
+        two = accum[slot * 2 + 1, 0:wide] * (1.0 / accum[slot * 2 + 1, wide : wide + 1])
+        contrast = one - lam[0:1, 0:1] * two
+        square = jnp.mean(contrast * contrast, axis=0, keepdims=True)
+        contrast = jnp.transpose(contrast * lax.rsqrt(square + 1e-05)) * gain_ref[...]
+        done[slot] = contrast.astype(jnp.bfloat16)
+        for k in range(2):
+            @pl.when(slot == k)
+            def _(k=k):
+                for piece in handed[k]:
+                    launch(*piece)
+
+    for h in range(in_plane * (tp_size // 2)):
+        part = o_ref.at[:, pl.ds(h * wide, wide)]
+        pltpu.make_async_copy(part, part, o_recv.at[h]).wait()
+
+    for here, far, near in pieces + handed[0] + handed[1]:
+        @pl.when(jnp.logical_not(here))
+        def _(far=far):
+            far.wait_send()
+
+    @pl.when(is_source)
+    def _():
+        lam_copy().wait_send()
+
+        @pl.loop(0, n)
+        def _(w):
+            s, r = source_of(w)
+            for which in range(2):
+                to_core(s, which).wait_send()
+
+                @pl.when(r == 0)
+                def _(which=which):
+                    for k in range(1, group):
+                        sideways(s, k, which).wait_send()
 
 
 def attention(queries, key_rows, value_rows, lambdas, head_gain):
     n = lax.axis_size("sp")
-    across_x = 2 ** (int(math.log2(n)) // 2)
+    tp_size = lax.axis_size("tp")
     length, columns = queries.shape
     wide = 2 * DH
     heads = columns // wide
+    group = n // (2 * heads)
+    chunks = 4 * group
+    size = length * n // chunks
+    post = length // tp_size
     kind = jnp.bfloat16
     dma = pltpu.SemaphoreType.DMA
-    deep = n // across_x
     vmem = pl.BlockSpec(memory_space=pltpu.VMEM)
     return pl.pallas_call(
-        functools.partial(attention_kernel, n, across_x, heads, math.gcd(length, 256)),
-        out_shape=jax.ShapeDtypeStruct((length, columns), kind),
-        in_specs=[vmem, pl.BlockSpec(memory_space=pl.ANY), vmem, vmem],
+        functools.partial(attention_kernel, n, group, heads, post),
+        out_shape=jax.ShapeDtypeStruct((post, columns * tp_size), kind),
+        in_specs=[vmem] * 5,
         out_specs=vmem,
         scratch_shapes=[
-            pltpu.VMEM((n, length, 2 * columns), kind),
-            pltpu.VMEM((2 * heads, length, wide), kind),
-            pltpu.VMEM((2 * heads, length, wide), jnp.float32),
-            pltpu.VMEM((2 * heads, length, 2 * wide), jnp.float32),
-            dma((1,)),
-            dma((deep + 1,)),
-            dma((deep + 1,)),
+            pltpu.VMEM((n, length, wide), kind),
+            pltpu.VMEM((n, wide, length), kind),
+            pltpu.VMEM((heads, wide, length), kind),
+            pltpu.VMEM((2, size, wide), kind),
+            pltpu.VMEM((4, 2 * wide, size), kind),
+            pltpu.VMEM((4, 8, size), jnp.float32),
+            pltpu.VMEM((4, wide + 16, size), jnp.float32),
+            pltpu.VMEM((2, size, wide), kind),
+            pltpu.VMEM((8, wide), jnp.float32),
+            dma((2 * heads,)),
             dma((n,)),
             dma((n,)),
+            dma((n, group, 2)),
+            dma((n, 2)),
+            dma((heads * chunks // n,)),
+            dma((2,)),
+            dma((1,)),
+            dma((1,)),
+            dma((2 * (size // post),)),
+            dma((heads * tp_size,)),
         ],
         compiler_params=pltpu.CompilerParams(
             collective_id=1, has_side_effects=True, vmem_limit_bytes=60000000
         ),
     )(
         queries,
-        jnp.concatenate([key_rows, value_rows], axis=1),
-        jnp.broadcast_to(lambdas[:, None], (heads, wide)),
+        key_rows,
+        value_rows,
+        jnp.broadcast_to(lambdas[:, None, None], (heads, 8, wide)),
         head_gain[None, :],
     )
 
@@ -516,8 +662,7 @@
     up_weight,
     down_weight,
 ):
-    heads_out = attention(queries, key_rows, value_rows, lambdas, head_gain)
-    heads_local = lax.all_to_all(heads_out, "tp", split_axis=0, concat_axis=1, tiled=True)
+    heads_local = attention(queries, key_rows, value_rows, lambdas, head_gain)
     attended = stream.astype(jnp.float32) + jnp.dot(
         heads_local, out_weight, preferred_element_type=jnp.float32
     )

time: 307 us -> 265 us (0.86)
  Pallas kernels: 277 us -> 246 us
  starting transfers between devices: 3.65 us -> 0 us
    pallas_call x1, Pallas kernels: 248 us -> 165 us  [exchange_and_apply(): pl.pallas_call(functools.partial(moe_kernel, n, lanes, slots), out_shape=...]
    pallas_call x1, Pallas kernels: 29.6 us -> 80.8 us  [attention(): pl.pallas_call(functools.partial(attention_kernel, n, group, heads, post)...]
    all_to_all x1 -> x0, starting transfers between devices: 3.65 us -> none  [local(): lax.all_to_all(heads_out, 'tp', split_axis=0, concat_axis=1, tiled=True)]
  transfers between devices with their start and end apart: 1 -> 0, of which waited for: 1 -> 0; matrix products, arithmetic and copies ran while one was open for 2% -> 0% of each run, Pallas kernels for 0% -> 0%
where the time goes in v1:
time: 265 us
  Pallas kernels  246 us (93%)
  matrix products  13.2 us (5%)
  local copies, waits for them, and re-layouts  3.11 us (1%)
    pallas_call x1, Pallas kernels, exchange_and_apply(): pl.pallas_call(functools.partial(moe_kernel, n, lanes, slots), out_shape=...  165 us
    pallas_call x1, Pallas kernels, attention(): pl.pallas_call(functools.partial(attention_kernel, n, group, heads, post)...  80.8 us

profile of v1, /device:TPU:0, one launch (start us, length us, event | category | flops | bytes accessed | tf_op | source)
XLA Modules:
  0.0 264.8 jit_solution(12792237605390133079)
XLA Ops:
  0.0 0.9 copy.24
  0.9 0.1 eq.44
  1.1 1.1 reduce-window.6
  2.2 0.2 slice_reduce_fusion
  2.5 0.1 eq.40
  2.6 0.1 fusion.9
  2.7 0.1 reduce_sum.30
  2.9 0.1 copy.26
  2.9 0.7 multiply_add_fusion
  3.6 0.2 convert_reduce_fusion
  3.8 1.3 broadcast_in_dim.4.lam_ref
  5.2 80.8 %shard_map.127 = bf16[256,1024]{1,0:T(8,128)(2,1)} custom-call(bf16[1024,256]{1,0:T(8,128)(2,1)} %q_ref.1, bf16[1024,256]{1,0:T(8,128)(2,1)} %k_ref.1, bf16[1024,256]{1,0:T(8,128)(2,1)} %v_ref.1, f32[2,8,128]{2,1,0:T(8,128)} %broadcast_in_dim.4.lam_ref, f32[1,128]{1,0:T(1,128)} %bitcast.26), custom_call_target="tpu_custom_call" | custom-call | tf_op jit(solution)/shard_map/pallas_call | solution.py:611
  85.9 0.0 copy-done.5
  86.0 0.0 copy-start.3
  86.0 3.8 %multiply_reduce_fusion = (f32[256]{0:T(256)S(1)}, f32[256,2048]{1,0:T(8,128)S(1)}) fusion(bf16[256,1024]{1,0:T(8,128)(2,1)} %shard_map.127, bf16[1024,2048]{1,0:T(8,128)(2,1)} %param.18, bf16[256,2048]{1,0:T(8,128)(2,1)S(1)} %copy-done.5), kind=kOutput, calls=%fused_computation.7 | convolution fusion | flops 1075838720 | bytes 7865344 | tf_op jit(solution)/shard_map/dot_general | solution.py:666
  89.7 0.0 copy-done.3
  89.7 2.5 convolution_convert_fusion
  92.3 0.0 copy-done
  92.3 165.2 %shard_map.128 = bf16[8,80,2048]{2,1,0:T(8,128)(2,1)} custom-call(bf16[8,80,2048]{2,1,0:T(8,128)(2,1)} %bitcast.24, bf16[2048,1280]{1,0:T(8,128)(2,1)} %bitcast.27, bf16[2048,1280]{1,0:T(8,128)(2,1)} %bitcast.28, bf16[1280,2048]{1,0:T(8,128)(2,1)} %bitcast.29), custom_call_target="tpu_custom_call" | custom-call | flops 40265318400 | bytes 15728640 | tf_op jit(solution)/shard_map/pallas_call | solution.py:253
  257.5 0.2 iota_compare_fusion
  257.7 0.0 copy-done.4
  257.7 0.1 copy.28
  257.9 3.2 %fusion = f32[256,1,640]{2,1,0:T(1,128)S(1)} fusion(f32[256,2,1]{1,2,0:T(1,128)S(1)} %copy.28, pred[256,2,640]{2,0,1:T(32,128)(4,1)S(1)} %iota_compare_fusion), kind=kOutput, calls=%fused_computation.2 | convolution fusion | flops 3932160 | bytes 985088 | tf_op jit(solution)/shard_map/tk,tks->ts/dot_general | solution.py:693
  261.1 3.7 %fusion.2 = bf16[256,2048]{1,0:T(8,128)(2,1)} fusion(f32[256,2048]{1,0:T(8,128)S(1)} %copy-done.1, bf16[640,2048]{1,0:T(8,128)(2,1)S(1)} %bitcast.23, f32[256,1,640]{2,1,0:T(1,128)S(1)} %fusion), kind=kOutput, calls=%fused_computation.5 | convolution fusion | flops 4027580416 | bytes 6422528 | tf_op jit(solution)/shard_map/dot_general | solution.py:705
  (11 shorter events, 0.1 us)
Async XLA Ops:
  0.0 85.9 %copy-start.5 = (bf16[256,2048]{1,0:T(8,128)(2,1)S(1)}, bf16[256,2048]{1,0:T(8,128)(2,1)}, u32[]{:S(2)}) copy-start(bf16[256,2048]{1,0:T(8,128)(2,1)} %param.19) | copy-start | bytes 3145732
  86.0 3.8 %copy-start.3 = (f32[2048]{0:T(1024)S(1)}, f32[2048]{0:T(1024)}, u32[]{:S(2)}) copy-start(f32[2048]{0:T(1024)} %param.20) | copy-start | bytes 24580
  89.7 2.5 copy-start
  92.3 165.5 %copy-start.4 = (f32[256,2]{0,1:T(2,128)S(1)}, f32[256,2]{0,1:T(2,128)}, u32[]{:S(2)}) copy-start(f32[256,2]{0,1:T(2,128)} %param.22) | copy-start | bytes 6148
  257.9 3.3 %copy-start.1 = (f32[256,2048]{1,0:T(8,128)S(1)}, f32[256,2048]{1,0:T(8,128)}, u32[]{:S(2)}) copy-start(f32[256,2048]{1,0:T(8,128)} %copy-done) | copy-start | bytes 6291460
  257.9 3.3 %copy-start.2 = (bf16[8,80,2048]{2,1,0:T(8,128)(2,1)S(1)}, bf16[8,80,2048]{2,1,0:T(8,128)(2,1)}, u32[]{:S(2)}) copy-start(bf16[8,80,2048]{2,1,0:T(8,128)(2,1)} %shard_map.128) | copy-start | bytes 7864324

commit v2 on v1

--- a/solution.py
+++ b/solution.py
@@ -71,8 +71,21 @@
             device_id_type=pl.DeviceIdType.MESH,
         )
 
+    near = n // 2
+
+    def order(i):
+        return i
+
+    def partner(k):
+        goal = 0
+        bit = 1
+        while bit < n:
+            goal = goal + (sp // bit + k // bit) % 2 * bit
+            bit *= 2
+        return goal
+
     def exchange(k):
-        goal = (sp + k) % n
+        goal = partner(k)
         return remote(out_ref.at[goal], block(k, 0, 0), a_send.at[k], a_recv.at[k], (goal, tp))
 
     def across(k, j):
@@ -85,9 +98,10 @@
             block(k, 0, j), block(k, 1, j), c_send.at[k, j], c_recv.at[k, j], (sp, other)
         )
 
-    def core_part(k):
+    def core_part(i):
+        k = order(i)
         return remote(
-            part.at[k % 2, pl.ds(half, half)], from_core.at[k], p_send.at[k], p_recv.at[k], (sp, other)
+            part.at[i % 2, pl.ds(half, half)], from_core.at[k], p_send.at[k], p_recv.at[k], (sp, other)
         )
 
     def y_part(k, j):
@@ -100,7 +114,7 @@
         )
 
     def give_back(k):
-        goal = (sp + n - k) % n
+        goal = partner(k)
         return remote(final.at[k], back_ref.at[sp], r_send.at[k], r_recv.at[k], (goal, tp))
 
     weights = [
@@ -141,92 +155,127 @@
     tile = math.gcd(gate.shape[1], 256)
     wide = math.gcd(down.shape[1], 256)
 
+    def enter(i):
+        k = order(i)
+        exchange(k).wait_recv()
+        forward(k)
+
+    def spread(i):
+        k = order(i)
+        for j in range(1, lanes):
+            across(k, j).wait_recv()
+            relay(k, j).start()
+
+    def compute(i):
+        k = order(i)
+
+        @pl.when(i == 0)
+        def _():
+            for copy in weights:
+                copy.wait()
+
+        for j in range(lanes):
+            relay(k, j).wait_recv()
+
+        @pl.when(i >= 2)
+        def _():
+            core_part(i - 2).wait_send()
+
+        @pl.loop(0, gate.shape[1] // tile)
+        def _(f):
+            cols = pl.ds(pl.multiple_of(f * tile, tile), tile)
+            x = rows[k]
+            g = jnp.dot(x, gate[:, cols], preferred_element_type=jnp.float32)
+            u = jnp.dot(x, up[:, cols], preferred_element_type=jnp.float32)
+            act[:, cols] = (g / (1.0 + jnp.exp(-g)) * u).astype(jnp.bfloat16)
+
+        @pl.loop(0, down.shape[1] // wide)
+        def _(d):
+            cols = pl.ds(pl.multiple_of(d * wide, wide), wide)
+            part[i % 2, :, cols] = jnp.dot(
+                act[...], down[:, cols], preferred_element_type=jnp.float32
+            ).astype(jnp.bfloat16)
+
+        core_part(i).start()
+
+    def reduce(i):
+        k = order(i)
+        core_part(i).wait_recv()
+
+        @pl.loop(0, half // 16)
+        def _(r):
+            at = pl.ds(pl.multiple_of(r * 16, 16), 16)
+            total = part[i % 2, at].astype(jnp.float32) + from_core[k, at].astype(jnp.float32)
+            chip_sum[k, at] = total.astype(jnp.bfloat16)
+
+    def cross(i):
+        for j in range(1, lanes):
+            y_part(order(i), j).start()
+
+    def finish(i):
+        k = order(i)
+        for j in range(1, lanes):
+            y_part(k, j).wait_recv()
+
+        @pl.loop(0, slots // 16)
+        def _(r):
+            at = pl.ds(pl.multiple_of(r * 16, 16), 16)
+            total = chip_sum[k, at].astype(jnp.float32)
+            for j in range(1, lanes):
+                here = pl.ds(pl.multiple_of((j - 1) * slots + r * 16, 16), 16)
+                total = total + from_y[k, here].astype(jnp.float32)
+            final[k, at] = total.astype(jnp.bfloat16)
+
+        @pl.when(k > 0)
+        def _():
+            give_back(k).start()
+
+        @pl.when(k == 0)
+        def _():
+            pltpu.make_async_copy(final.at[0], back_ref.at[sp], local_sem.at[1]).start()
+
+    def urgent(i):
+        return (i == 0) | (i >= near)
+
     @pl.loop(0, n + 3)
     def _(i):
         @pl.when(i < n - 1)
         def _():
-            exchange(i + 1).wait_recv()
-            forward(i + 1)
+            enter(i + 1)
 
         @pl.when(i < n)
         def _():
-            for j in range(1, lanes):
-                across(i, j).wait_recv()
-                relay(i, j).start()
+            spread(i)
 
         @pl.when((i >= 1) & (i < n + 1))
         def _():
-            k = i - 1
-
-            @pl.when(k == 0)
+            compute(i - 1)
+
+        @pl.when((i >= 2) & (i < n + 2))
+        def _():
+            reduce(i - 2)
+
+            @pl.when(urgent(i - 2))
             def _():
-                for copy in weights:
-                    copy.wait()
-
-            for j in range(lanes):
-                relay(k, j).wait_recv()
-
-            @pl.when(k >= 2)
-            def _():
-                core_part(k - 2).wait_send()
-
-            @pl.loop(0, gate.shape[1] // tile)
-            def _(f):
-                cols = pl.ds(pl.multiple_of(f * tile, tile), tile)
-                x = rows[k]
-                g = jnp.dot(x, gate[:, cols], preferred_element_type=jnp.float32)
-                u = jnp.dot(x, up[:, cols], preferred_element_type=jnp.float32)
-                act[:, cols] = (g / (1.0 + jnp.exp(-g)) * u).astype(jnp.bfloat16)
-
-            @pl.loop(0, down.shape[1] // wide)
-            def _(d):
-                cols = pl.ds(pl.multiple_of(d * wide, wide), wide)
-                part[k % 2, :, cols] = jnp.dot(
-                    act[...], down[:, cols], preferred_element_type=jnp.float32
-                ).astype(jnp.bfloat16)
-
-            core_part(k).start()
-
-        @pl.when((i >= 2) & (i < n + 2))
-        def _():
-            k = i - 2
-            core_part(k).wait_recv()
-
-            @pl.loop(0, half // 16)
-            def _(r):
-                at = pl.ds(pl.multiple_of(r * 16, 16), 16)
-                total = part[k % 2, at].astype(jnp.float32) + from_core[k, at].astype(jnp.float32)
-                chip_sum[k, at] = total.astype(jnp.bfloat16)
-
-            for j in range(1, lanes):
-                y_part(k, j).start()
-
-        @pl.when(i >= 3)
-        def _():
-            k = i - 3
-            for j in range(1, lanes):
-                y_part(k, j).wait_recv()
-
-            @pl.loop(0, slots // 16)
-            def _(r):
-                at = pl.ds(pl.multiple_of(r * 16, 16), 16)
-                total = chip_sum[k, at].astype(jnp.float32)
-                for j in range(1, lanes):
-                    here = pl.ds(pl.multiple_of((j - 1) * slots + r * 16, 16), 16)
-                    total = total + from_y[k, here].astype(jnp.float32)
-                final[k, at] = total.astype(jnp.bfloat16)
-
-            @pl.when(k > 0)
-            def _():
-                give_back(k).start()
-
-            @pl.when(k == 0)
-            def _():
-                pltpu.make_async_copy(final.at[0], back_ref.at[sp], local_sem.at[1]).start()
+                cross(i - 2)
+
+        @pl.when(i == n + 1)
+        def _():
+            @pl.loop(1, near)
+            def _(k):
+                cross(k)
+
+        @pl.when((i >= 3) & urgent(i - 3))
+        def _():
+            finish(i - 3)
+
+    @pl.loop(1, near)
+    def _(k):
+        finish(k)
 
     pltpu.make_async_copy(final.at[0], back_ref.at[sp], local_sem.at[1]).wait()
-    for k in (n - 2, n - 1):
-        core_part(k).wait_send()
+    for i in (n - 2, n - 1):
+        core_part(i).wait_send()
 
     @pl.loop(0, n)
     def _(k):
@@ -515,19 +564,28 @@
         def _():
             attend(slot, s, chunk, False)
 
+    def slot_of(i):
+        return jnp.where(2 * sp < n, 1 - i, i)
+
+    rounds = n // group
+
     receive(0)
 
-    @pl.loop(0, n)
-    def _(w):
-        @pl.when(w + 1 < n)
-        def _():
-            receive(w + 1)
-
-        @pl.when(w < n - group)
-        def _():
-            @pl.loop(0, 2)
-            def _(slot):
-                step(slot, w)
+    @pl.loop(0, rounds)
+    def _(t):
+        @pl.loop(0, group)
+        def _(r):
+            @pl.when(r > 0)
+            def _():
+                receive(t * group + r)
+
+            @pl.when((r == group - 1) & (t < rounds - 1))
+            def _():
+                receive((t + 1) * group)
+
+            @pl.loop(0, jnp.where(t < rounds - 1, 2, 1))
+            def _(i):
+                step(slot_of(i), t * group + r)
 
     @pl.when(is_source)
     def _():
@@ -553,10 +611,14 @@
     handed = [[hand_over(slot, i) for i in range(parts)] for slot in range(2)]
 
     @pl.loop(0, 2)
-    def _(slot):
-        @pl.loop(n - group, n)
-        def _(w):
-            step(slot, w)
+    def _(i):
+        slot = slot_of(i)
+
+        @pl.when(i == 1)
+        def _():
+            @pl.loop(n - group, n)
+            def _(w):
+                step(slot, w)
 
         one = accum[slot * 2, 0:wide] * (1.0 / accum[slot * 2, wide : wide + 1])
         two = accum[slot * 2 + 1, 0:wide] * (1.0 / accum[slot * 2 + 1, wide : wide + 1])

time: 265 us -> 245 us (0.925)
  Pallas kernels: 246 us -> 225 us
    pallas_call x1, Pallas kernels: 80.8 us -> 68.5 us  [attention(): pl.pallas_call(functools.partial(attention_kernel, n, group, heads, post)...]
    pallas_call x1, Pallas kernels: 165 us -> 157 us  [exchange_and_apply(): pl.pallas_call(functools.partial(moe_kernel, n, lanes, slots), out_shape=...]
where the time goes in v2:
time: 245 us; the launch traced here: 244 us
  Pallas kernels  225 us (92%)
  matrix products  13.2 us (5%)
  local copies, waits for them, and re-layouts  3.11 us (1%)
    pallas_call x1, Pallas kernels, exchange_and_apply(): pl.pallas_call(functools.partial(moe_kernel, n, lanes, slots), out_shape=...  157 us
    pallas_call x1, Pallas kernels, attention(): pl.pallas_call(functools.partial(attention_kernel, n, group, heads, post)...  68.5 us

profile of v2, /device:TPU:0, one launch (start us, length us, event | category | flops | bytes accessed | tf_op | source)
XLA Modules:
  0.0 243.9 jit_solution(1078576848715912343)
XLA Ops:
  0.0 0.9 copy.24
  0.9 0.1 eq.44
  1.1 1.1 reduce-window.6
  2.2 0.2 slice_reduce_fusion
  2.5 0.1 eq.40
  2.6 0.1 fusion.9
  2.7 0.1 reduce_sum.30
  2.9 0.1 copy.26
  2.9 0.7 multiply_add_fusion
  3.6 0.2 convert_reduce_fusion
  3.8 1.3 broadcast_in_dim.4.lam_ref
  5.2 68.5 %shard_map.127 = bf16[256,1024]{1,0:T(8,128)(2,1)} custom-call(bf16[1024,256]{1,0:T(8,128)(2,1)} %q_ref.1, bf16[1024,256]{1,0:T(8,128)(2,1)} %k_ref.1, bf16[1024,256]{1,0:T(8,128)(2,1)} %v_ref.1, f32[2,8,128]{2,1,0:T(8,128)} %broadcast_in_dim.4.lam_ref, f32[1,128]{1,0:T(1,128)} %bitcast.26), custom_call_target="tpu_custom_call" | custom-call | tf_op jit(solution)/shard_map/pallas_call | solution.py:673
  73.7 0.0 copy-done.5
  73.7 0.0 copy-start.3
  73.7 3.8 %multiply_reduce_fusion = (f32[256]{0:T(256)S(1)}, f32[256,2048]{1,0:T(8,128)S(1)}) fusion(bf16[256,1024]{1,0:T(8,128)(2,1)} %shard_map.127, bf16[1024,2048]{1,0:T(8,128)(2,1)} %param.18, bf16[256,2048]{1,0:T(8,128)(2,1)S(1)} %copy-done.5), kind=kOutput, calls=%fused_computation.7 | convolution fusion | flops 1075838720 | bytes 7865344 | tf_op jit(solution)/shard_map/dot_general | solution.py:728
  77.5 0.0 copy-done.3
  77.5 2.5 %convolution_convert_fusion = bf16[640,2048]{1,0:T(8,128)(2,1)} fusion(f32[256,2048]{1,0:T(8,128)S(1)} %get-tuple-element.6, f32[2048]{0:T(1024)S(1)} %copy-done.3, f32[256]{0:T(256)S(1)} %add_rsqrt_fusion, bf16[256,640]{1,0:T(8,128)(2,1)S(1)} %convert_reduce_fusion), kind=kOutput, calls=%fused_computation | convolution fusion | flops 673972224 | bytes 5055488 | tf_op jit(solution)/shard_map/dot_general | solution.py:757
  80.0 0.0 copy-done
  80.0 156.5 %shard_map.128 = bf16[8,80,2048]{2,1,0:T(8,128)(2,1)} custom-call(bf16[8,80,2048]{2,1,0:T(8,128)(2,1)} %bitcast.24, bf16[2048,1280]{1,0:T(8,128)(2,1)} %bitcast.27, bf16[2048,1280]{1,0:T(8,128)(2,1)} %bitcast.28, bf16[1280,2048]{1,0:T(8,128)(2,1)} %bitcast.29), custom_call_target="tpu_custom_call" | custom-call | flops 40265318400 | bytes 15728640 | tf_op jit(solution)/shard_map/pallas_call | solution.py:302
  236.5 0.2 iota_compare_fusion
  236.8 0.0 copy-done.4
  236.8 0.1 copy.28
  237.0 3.2 %fusion = f32[256,1,640]{2,1,0:T(1,128)S(1)} fusion(f32[256,2,1]{1,2,0:T(1,128)S(1)} %copy.28, pred[256,2,640]{2,0,1:T(32,128)(4,1)S(1)} %iota_compare_fusion), kind=kOutput, calls=%fused_computation.2 | convolution fusion | flops 3932160 | bytes 985088 | tf_op jit(solution)/shard_map/tk,tks->ts/dot_general | solution.py:755
  240.2 3.7 %fusion.2 = bf16[256,2048]{1,0:T(8,128)(2,1)} fusion(f32[256,2048]{1,0:T(8,128)S(1)} %copy-done.1, bf16[640,2048]{1,0:T(8,128)(2,1)S(1)} %bitcast.23, f32[256,1,640]{2,1,0:T(1,128)S(1)} %fusion), kind=kOutput, calls=%fused_computation.5 | convolution fusion | flops 4027580416 | bytes 6422528 | tf_op jit(solution)/shard_map/dot_general | solution.py:767
  (11 shorter events, 0.1 us)
Async XLA Ops:
  0.0 73.7 %copy-start.5 = (bf16[256,2048]{1,0:T(8,128)(2,1)S(1)}, bf16[256,2048]{1,0:T(8,128)(2,1)}, u32[]{:S(2)}) copy-start(bf16[256,2048]{1,0:T(8,128)(2,1)} %param.19) | copy-start | bytes 3145732
  73.7 3.8 %copy-start.3 = (f32[2048]{0:T(1024)S(1)}, f32[2048]{0:T(1024)}, u32[]{:S(2)}) copy-start(f32[2048]{0:T(1024)} %param.20) | copy-start | bytes 24580
  77.4 2.5 %copy-start = (f32[256,2048]{1,0:T(8,128)}, f32[256,2048]{1,0:T(8,128)S(1)}, u32[]{:S(2)}) copy-start(f32[256,2048]{1,0:T(8,128)S(1)} %get-tuple-element.6) | copy-start | bytes 6291460
  80.0 156.8 %copy-start.4 = (f32[256,2]{0,1:T(2,128)S(1)}, f32[256,2]{0,1:T(2,128)}, u32[]{:S(2)}) copy-start(f32[256,2]{0,1:T(2,128)} %param.22) | copy-start | bytes 6148
  236.9 3.3 %copy-start.1 = (f32[256,2048]{1,0:T(8,128)S(1)}, f32[256,2048]{1,0:T(8,128)}, u32[]{:S(2)}) copy-start(f32[256,2048]{1,0:T(8,128)} %copy-done) | copy-start | bytes 6291460
  237.0 3.3 %copy-start.2 = (bf16[8,80,2048]{2,1,0:T(8,128)(2,1)S(1)}, bf16[8,80,2048]{2,1,0:T(8,128)(2,1)}, u32[]{:S(2)}) copy-start(bf16[8,80,2048]{2,1,0:T(8,128)(2,1)} %shard_map.128) | copy-start | bytes 7864324

commit v3 on v2

--- a/solution.py
+++ b/solution.py
@@ -19,7 +19,13 @@
     gate_hbm,
     up_hbm,
     down_hbm,
+    stream_ref,
+    spot_ref,
+    share_ref,
+    o_ref,
     back_ref,
+    total_ref,
+    share_cols,
     gate,
     up,
     down,
@@ -151,6 +157,7 @@
 
     own.wait()
     forward(0)
+    total_ref[...] = stream_ref[...]
 
     tile = math.gcd(gate.shape[1], 256)
     wide = math.gcd(down.shape[1], 256)
@@ -234,6 +241,27 @@
         def _():
             pltpu.make_async_copy(final.at[0], back_ref.at[sp], local_sem.at[1]).start()
 
+    rows_here = spot_ref.shape[0]
+    top_count = spot_ref.shape[1]
+    shares = jnp.transpose(jnp.concatenate([share_ref[...]] * (8 // top_count), axis=0))
+    share_cols[...] = jnp.concatenate([shares] * 16, axis=1)
+
+    def gather(e):
+        lane = e * slots + lax.broadcasted_iota(jnp.int32, (rows_here, slots), 1)
+        hits = [
+            (spot_ref[:, c : c + 1] == lane).astype(jnp.float32).astype(jnp.bfloat16)
+            for c in range(spot_ref.shape[1])
+        ]
+
+        @pl.loop(0, down.shape[1] // wide)
+        def _(d):
+            cols = pl.ds(pl.multiple_of(d * wide, wide), wide)
+            total = total_ref[:, cols]
+            for c, hit in enumerate(hits):
+                row = jnp.dot(hit, back_ref[e, :, cols], preferred_element_type=jnp.float32)
+                total = total + share_cols[:, c : c + 1] * row
+            total_ref[:, cols] = total
+
     def urgent(i):
         return (i == 0) | (i >= near)
 
@@ -274,6 +302,22 @@
         finish(k)
 
     pltpu.make_async_copy(final.at[0], back_ref.at[sp], local_sem.at[1]).wait()
+
+    @pl.loop(0, n)
+    def _(i):
+        k = i // 2 + i % 2 * near
+
+        @pl.when(k > 0)
+        def _():
+            give_back(k).wait_recv()
+
+        gather(partner(k))
+
+    @pl.loop(0, down.shape[1] // wide)
+    def _(d):
+        cols = pl.ds(pl.multiple_of(d * wide, wide), wide)
+        o_ref[:, cols] = total_ref[:, cols].astype(jnp.bfloat16)
+
     for i in (n - 2, n - 1):
         core_part(i).wait_send()
 
@@ -283,7 +327,6 @@
         def _():
             exchange(k).wait_send()
             give_back(k).wait_send()
-            give_back(k).wait_recv()
 
         for j in range(1, lanes):
             across(k, j).wait_send()
@@ -292,7 +335,7 @@
             relay(k, j).wait_send()
 
 
-def exchange_and_apply(outgoing, gate_local, up_local, down_local):
+def exchange_and_apply(outgoing, gate_local, up_local, down_local, attended, spots, shares):
     n, slots, width = outgoing.shape
     lanes = lax.axis_size("tp") // 2
     hidden = gate_local.shape[1]
@@ -301,11 +344,15 @@
     flops = 6 * n * lanes * 2 * slots * width * hidden
     return pl.pallas_call(
         functools.partial(moe_kernel, n, lanes, slots),
-        out_shape=jax.ShapeDtypeStruct((n, slots, width), kind),
+        out_shape=jax.ShapeDtypeStruct(attended.shape, kind),
         in_specs=[pl.BlockSpec(memory_space=pltpu.VMEM)]
-        + [pl.BlockSpec(memory_space=pl.ANY)] * 3,
+        + [pl.BlockSpec(memory_space=pl.ANY)] * 3
+        + [pl.BlockSpec(memory_space=pltpu.VMEM)] * 3,
         out_specs=pl.BlockSpec(memory_space=pltpu.VMEM),
         scratch_shapes=[
+            pltpu.VMEM((n, slots, width), kind),
+            pltpu.VMEM(attended.shape, jnp.float32),
+            pltpu.VMEM((attended.shape[0], 128), jnp.float32),
             pltpu.VMEM((width, hidden), kind),
             pltpu.VMEM((width, hidden), kind),
             pltpu.VMEM((hidden, width), kind),
@@ -337,7 +384,7 @@
         cost_estimate=pl.CostEstimate(
             flops=flops, bytes_accessed=6 * width * hidden, transcendentals=0
         ),
-    )(outgoing, gate_local, up_local, down_local)
+    )(outgoing, gate_local, up_local, down_local, attended, spots, shares)
 
 
 def attention_kernel(
@@ -360,6 +407,7 @@
     accum,
     done,
     lam,
+    lam_out,
     kv_send,
     k_recv,
     v_recv,
@@ -416,6 +464,7 @@
             device_id_type=pl.DeviceIdType.MESH,
         )
 
+    lam_out[...] = jnp.full(lam_out.shape, lam_ref[head % heads], jnp.float32)
     pl.semaphore_wait(barrier, everyone - 1)
 
     def columns(h):
@@ -480,7 +529,7 @@
 
     def lam_copy():
         return remote(
-            lam_ref.at[head % heads], lam, lam_send.at[0], lam_recv.at[0], (sp, other)
+            lam_out, lam, lam_send.at[0], lam_recv.at[0], (sp, other)
         )
 
     @pl.when(is_source)
@@ -589,7 +638,7 @@
 
     @pl.when(is_source)
     def _():
-        lam[...] = lam_ref[head % heads]
+        lam[...] = lam_out[...]
 
     @pl.when(jnp.logical_not(is_source))
     def _():
@@ -673,7 +722,7 @@
     return pl.pallas_call(
         functools.partial(attention_kernel, n, group, heads, post),
         out_shape=jax.ShapeDtypeStruct((post, columns * tp_size), kind),
-        in_specs=[vmem] * 5,
+        in_specs=[vmem] * 3 + [pl.BlockSpec(memory_space=pltpu.SMEM), vmem],
         out_specs=vmem,
         scratch_shapes=[
             pltpu.VMEM((n, length, wide), kind),
@@ -684,6 +733,7 @@
             pltpu.VMEM((4, 8, size), jnp.float32),
             pltpu.VMEM((4, wide + 16, size), jnp.float32),
             pltpu.VMEM((2, size, wide), kind),
+            pltpu.VMEM((8, wide), jnp.float32),
             pltpu.VMEM((8, wide), jnp.float32),
             dma((2 * heads,)),
             dma((n,)),
@@ -704,7 +754,7 @@
         queries,
         key_rows,
         value_rows,
-        jnp.broadcast_to(lambdas[:, None, None], (heads, 8, wide)),
+        lambdas,
         head_gain[None, :],
     )
 
@@ -752,7 +802,6 @@
     )
     placed = placed.reshape(rows_local, top_count, experts * slots)
     dispatch = jnp.transpose(jnp.sum(placed, axis=1)).astype(jnp.bfloat16)
-    combine = jnp.einsum("tk,tks->ts", route_weight, placed, precision=lax.Precision.HIGHEST)
     outgoing = (
         jnp.dot(dispatch, normed, preferred_element_type=jnp.float32)
         .astype(jnp.bfloat16)
@@ -761,11 +810,15 @@
     gate_local = gate_weight[0]
     up_local = up_weight[0]
     down_local = down_weight[0]
-    returned = exchange_and_apply(outgoing, gate_local, up_local, down_local).reshape(
-        experts * slots, width
+    return exchange_and_apply(
+        outgoing,
+        gate_local,
+        up_local,
+        down_local,
+        attended,
+        target.reshape(rows_local, top_count),
+        route_weight.T,
     )
-    routed = jnp.dot(combine, returned.astype(jnp.float32), precision=lax.Precision.HIGHEST)
-    return (attended + routed).astype(jnp.bfloat16)
 
 
 def solution(mesh):

time: 245 us -> 243 us (level)
  matrix products: 13.2 us -> 6.24 us
  Pallas kernels: 225 us -> 230 us
    dot_general x2 -> x0, matrix products: 6.9 us -> none  [the longest x1 3.67 us: local(): jnp.dot(combine, returned.astype(jnp.float32), precision=lax.Precision.HI...]
    pallas_call x1, Pallas kernels: 157 us -> 161 us  [exchange_and_apply(): pl.pallas_call(functools.partial(moe_kernel, n, lanes, slots), out_shape=...]
where the time goes in v3:
time: 243 us; the launch traced here: 242 us
  Pallas kernels  230 us (95%)
  matrix products  6.24 us (3%)
  local copies, waits for them, and re-layouts  4 us (2%)
    pallas_call x1, Pallas kernels, exchange_and_apply(): pl.pallas_call(functools.partial(moe_kernel, n, lanes, slots), out_shape=...  161 us
    pallas_call x1, Pallas kernels, attention(): pl.pallas_call(functools.partial(attention_kernel, n, group, heads, post)...  68.7 us

profile of v3, /device:TPU:0, one launch (start us, length us, event | category | flops | bytes accessed | tf_op | source)
XLA Modules:
  0.0 242.4 jit_solution(17363716976791228622)
XLA Ops:
  0.0 0.0 copy-start.3
  0.0 0.8 broadcast_multiply_fusion
  0.8 0.1 copy.27
  0.9 0.8 copy.25
  1.7 0.1 eq.43
  1.9 0.1 eq.39
  2.0 1.1 reduce-window.6
  3.2 0.2 slice_reduce_fusion
  3.4 0.1 fusion.4
  3.5 0.1 reduce_sum.30
  3.7 0.0 copy-start.1
  3.7 0.1 copy.28
  3.8 0.2 convert_reduce_fusion
  4.0 68.7 %shard_map.127 = bf16[256,1024]{1,0:T(8,128)(2,1)} custom-call(bf16[1024,256]{1,0:T(8,128)(2,1)} %q_ref.1, bf16[1024,256]{1,0:T(8,128)(2,1)} %k_ref.1, bf16[1024,256]{1,0:T(8,128)(2,1)} %v_ref.1, f32[2]{0:T(128)} %lam_ref.1, f32[1,128]{1,0:T(1,128)} %bitcast.18), custom_call_target="tpu_custom_call" | custom-call | tf_op jit(solution)/shard_map/pallas_call | solution.py:722
  72.7 0.0 copy-done.3
  72.7 0.0 copy-start.2
  72.8 3.7 %multiply_reduce_fusion = (f32[256]{0:T(256)S(1)}, f32[256,2048]{1,0:T(8,128)S(1)}) fusion(bf16[256,1024]{1,0:T(8,128)(2,1)} %shard_map.127, bf16[1024,2048]{1,0:T(8,128)(2,1)} %param.18, bf16[256,2048]{1,0:T(8,128)(2,1)S(1)} %copy-done.3), kind=kOutput, calls=%fused_computation.3 | convolution fusion | flops 1075838720 | bytes 7865344 | tf_op jit(solution)/shard_map/dot_general | solution.py:778
  76.5 0.0 copy-done.1
  76.5 0.0 copy-start
  76.5 0.0 copy-done.2
  76.6 2.5 %convolution_convert_fusion = bf16[640,2048]{1,0:T(8,128)(2,1)} fusion(f32[256,2048]{1,0:T(8,128)S(1)} %get-tuple-element.6.stream_ref, f32[2048]{0:T(1024)S(1)} %copy-done.2, f32[256]{0:T(256)S(1)} %add_rsqrt_fusion, bf16[256,640]{1,0:T(8,128)(2,1)S(1)} %convert_reduce_fusion), kind=kOutput, calls=%fused_computation | convolution fusion | flops 673972224 | bytes 5055488 | tf_op jit(solution)/shard_map/dot_general | solution.py:806
  79.0 0.0 copy-done
  79.0 161.0 %shard_map.128 = bf16[256,2048]{1,0:T(8,128)(2,1)} custom-call(bf16[8,80,2048]{2,1,0:T(8,128)(2,1)} %bitcast.17, bf16[2048,1280]{1,0:T(8,128)(2,1)} %bitcast.19, bf16[2048,1280]{1,0:T(8,128)(2,1)} %bitcast.20, bf16[1280,2048]{1,0:T(8,128)(2,1)} %bitcast.21, f32[256,2048]{1,0:T(8,128)} %copy-done, s32[256,2]{1,0:T(8,128)} %copy-done.1, f32[2,256]{1,0:T(2,128)} %bitcast.22), custom_call_target="tpu_custom_call" | custom-call | flops 40265318400 | bytes 15728640 | tf_op jit(solution)/shard_map/pallas_call | solution.py:345
  240.1 2.3 copy.30
  (5 shorter events, 0.1 us)
Async XLA Ops:
  0.0 72.7 %copy-start.3 = (bf16[256,2048]{1,0:T(8,128)(2,1)S(1)}, bf16[256,2048]{1,0:T(8,128)(2,1)}, u32[]{:S(2)}) copy-start(bf16[256,2048]{1,0:T(8,128)(2,1)} %param.19) | copy-start | bytes 3145732
  3.7 72.8 %copy-start.1 = (s32[256,2]{1,0:T(8,128)}, s32[256,2]{1,0:T(8,128)S(1)}, u32[]{:S(2)}) copy-start(s32[256,2]{1,0:T(8,128)S(1)} %add.22.spot_ref) | copy-start | bytes 6148
  72.7 3.8 %copy-start.2 = (f32[2048]{0:T(1024)S(1)}, f32[2048]{0:T(1024)}, u32[]{:S(2)}) copy-start(f32[2048]{0:T(1024)} %param.20) | copy-start | bytes 24580
  76.5 2.5 %copy-start = (f32[256,2048]{1,0:T(8,128)}, f32[256,2048]{1,0:T(8,128)S(1)}, u32[]{:S(2)}) copy-start(f32[256,2048]{1,0:T(8,128)S(1)} %get-tuple-element.6.stream_ref) | copy-start | bytes 6291460
